TPU v7x, 32 devices: a whole 2x2x4 slice. The times are simulated.
32 devices in a mesh: fs: 8 (over z, core), tp: 4 (over y, x).
Axes of the slice: x: 2, y: 2, z: 4, core: 2. Of those that a mesh axis runs over, the one named last changes fastest.
Arguments:
- tokens: bfloat16 [2048, 2048], P('fs'), may hold values from -6 to 6
- routes: int32 [2048, 2], P('fs'), may hold values from 0 to 3, all different within a row
- route_logits: float32 [2048, 2], P('fs'), may hold values from -6 to 6
- norm_gain: float32 [2048], P('fs'), may hold values from 0.1 to 1.9
- gate_weight: float32 [2048, 8192], P('fs', 'tp')
- up_weight: float32 [2048, 8192], P('fs', 'tp')
- down_weight: float32 [2048, 8192], P('fs', 'tp'), may hold values from -0.125 to 0.125
Outputs:
- gate_sampler: bfloat16 [2048, 8192], P(None, 'tp')
- up_sampler: bfloat16 [2048, 8192], P(None, 'tp')
- down_sampler: bfloat16 [2048, 8192], P(None, 'tp')
- moe_out: bfloat16 [2048, 2048], P('fs', 'tp')
Inputs may be any that keep to these rules, and one draw needn't show every extreme that they name: `routes`: each row names 2 different experts; every expert is named by some row.
All inputs are finite; a program needn't handle non-finite values.
Results may differ from a plain program's by a relative error of at most 0.014.
Values may be sent and summed in bfloat16 or wider, within the bound.
A program may use at most 128 MiB of HBM per device.

v0:
```python
import jax
import jax.numpy as jnp
from jax import lax
from jax.sharding import PartitionSpec as P

FF = 2048


EPSILON = 1e-06
CLAMP_LIMIT = 7.0
SIGMOID_SCALE = 1.702


def clamped_unit(pre_gate, pre_up):
    gated = jnp.minimum(pre_gate, CLAMP_LIMIT)
    upper = jnp.clip(pre_up, -CLAMP_LIMIT, CLAMP_LIMIT)
    return gated * jax.nn.sigmoid(SIGMOID_SCALE * gated) * (upper + 1.0)


def on_device(tokens, routes, route_logits, norm_gain, gate_weight, up_weight, down_weight):
    hidden_cols = gate_weight.shape[1]
    gate_local = (norm_gain[:, None] * gate_weight).astype(jnp.bfloat16)
    up_local = (norm_gain[:, None] * up_weight).astype(jnp.bfloat16)
    down_local = down_weight.astype(jnp.bfloat16)
    widened = tokens.astype(jnp.float32)
    normed = (
        widened * lax.rsqrt(jnp.mean(widened * widened, axis=-1, keepdims=True) + EPSILON)
    ).astype(jnp.bfloat16)
    shares = jax.nn.softmax(route_logits, axis=-1)
    my_expert = lax.axis_index("tp") * hidden_cols // FF
    weight = jnp.sum(
        jnp.where(routes == my_expert, shares, jnp.float32(0.0)), axis=-1, keepdims=True
    )
    gate_full, up_full, down_full = (
        lax.all_gather(gate_local, "fs", axis=0, tiled=True),
        lax.all_gather(up_local, "fs", axis=0, tiled=True),
        lax.all_gather(down_local, "fs", axis=0, tiled=True),
    )
    pre_gate = jnp.dot(normed, gate_full, preferred_element_type=jnp.float32)
    pre_up = jnp.dot(normed, up_full, preferred_element_type=jnp.float32)
    active = (weight * clamped_unit(pre_gate, pre_up)).astype(jnp.bfloat16)
    shares_out = lax.psum_scatter(
        lax.dot_general(
            down_full, active, (((1,), (1,)), ((), ())), preferred_element_type=jnp.float32
        ).astype(jnp.bfloat16),
        "tp",
        scatter_dimension=0,
        tiled=True,
    ).astype(jnp.float32)
    moe_out = jnp.transpose(shares_out).astype(jnp.bfloat16)
    return (gate_full, up_full, down_full, moe_out)


def solution(mesh):
    return jax.shard_map(
        on_device,
        mesh=mesh,
        in_specs=(
            P("fs", None),
            P("fs", None),
            P("fs", None),
            P("fs"),
            P("fs", "tp"),
            P("fs", "tp"),
            P("fs", "tp"),
        ),
        out_specs=(P(None, "tp"), P(None, "tp"), P(None, "tp"), P("fs", "tp")),
        check_vma=False,
    )
```

profile of v0, /device:TPU:0, one launch (start us, length us, event | category | flops | bytes accessed | tf_op | source)
XLA Modules:
  0.0 332.1 jit_solution(6189443235585608303)
XLA Ops:
  7.2 0.0 all-gather.4.cloned.1.call-start
  7.2 4.2 %multiply_convert_fusion = (bf16[256,2048]{1,0:T(8,128)(2,1)}, bf16[256,2048]{1,0:T(8,128)(2,1)}) fusion(f32[256,2048]{1,0:T(8,128)} %param.12, f32[256]{0:T(256)} %param.10, f32[256,2048]{1,0:T(8,128)} %param.11), kind=kLoop, calls=%fused_computation.12 | loop fusion | flops 2097152 | bytes 6292480 | tf_op jit(solution)/shard_map/convert_element_type | solution.py:23
  11.4 0.0 copy-start
  11.4 0.0 all-gather.4.cloned.1.call-update
  11.4 0.0 all-gather.6.cloned.1.call-start
  11.4 0.7 all-gather.6.cloned.1.call-update
  12.1 0.0 copy-start.2
  12.2 0.0 copy-start.3
  12.2 0.0 copy-start.1
  12.2 0.0 all-gather.8.cloned.1.call-start
  12.2 0.7 copy-done
  13.0 1.1 convert_element_type.31
  14.1 0.0 all-gather.8.cloned.1.call-update
  14.1 0.0 reduce-scatter.2.cloned.1.call-start
  14.2 0.0 copy-done.2
  14.2 0.0 copy-done.3
  14.3 0.0 copy-done.1
  14.3 0.3 fusion.5
  14.6 81.7 %all-gather.4.cloned.1.call-done = bf16[2048,2048]{1,0:T(8,128)(2,1)} async-done(((bf16[256,2048]{1,0:T(8,128)(2,1)}), bf16[2048,2048]{1,0:T(8,128)(2,1)}) %all-gather.4.cloned.1.call-update) | async-done | bytes 8388624 | tf_op jit(solution)/shard_map/all_gather | solution.py:35
  96.3 5.8 %convolution_minimum_fusion = f32[256,2048]{1,0:T(8,128)S(1)} fusion(bf16[2048,2048]{1,0:T(8,128)(2,1)} %all-gather.4.cloned.1.call-done, bf16[256,2048]{1,0:T(8,128)(2,1)S(1)} %copy-done.1, f32[256]{0:T(256)S(1)} %add_rsqrt_fusion), kind=kOutput, calls=%fused_computation.1 | convolution fusion | flops 2149580800 | bytes 11535360 | tf_op jit(solution)/shard_map/dot_general | solution.py:39
  102.1 76.9 %all-gather.6.cloned.1.call-done = bf16[2048,2048]{1,0:T(8,128)(2,1)} async-done(((bf16[256,2048]{1,0:T(8,128)(2,1)}), bf16[2048,2048]{1,0:T(8,128)(2,1)}) %all-gather.6.cloned.1.call-update) | async-done | bytes 8388624 | tf_op jit(solution)/shard_map/all_gather | solution.py:36
  179.0 82.7 %all-gather.8.cloned.1.call-done = bf16[2048,2048]{1,0:T(8,128)(2,1)} async-done(((bf16[256,2048]{1,0:T(8,128)(2,1)}), bf16[2048,2048]{1,0:T(8,128)(2,1)}) %all-gather.8.cloned.1.call-update) | async-done | bytes 8388624 | tf_op jit(solution)/shard_map/all_gather | solution.py:37
  261.8 11.9 %fusion.4 = bf16[2048,256]{0,1:T(8,128)(2,1)} fusion(bf16[2048,2048]{1,0:T(8,128)(2,1)} %all-gather.8.cloned.1.call-done, bf16[2048,2048]{1,0:T(8,128)(2,1)} %all-gather.6.cloned.1.call-done, f32[256,2048]{1,0:T(8,128)S(1)} %convolution_minimum_fusion, f32[256]{0:T(256)S(1)} %fusion.10, bf16[256,2048]{1,0:T(8,128)(2,1)S(1)} %copy-done.1, ...), kind=kOutput, calls=%fused_computation.9 | convolution fusion | flops 4302307328 | bytes 20973568 | tf_op jit(solution)/shard_map/dot_general | solution.py:43
  273.6 0.0 reduce-scatter.2.cloned.1.call-update
  273.6 26.6 %reduce-scatter.2.cloned.1.call-done = bf16[512,256]{0,1:T(8,128)(2,1)} async-done(((bf16[2048,256]{0,1:T(8,128)(2,1)}), bf16[512,256]{0,1:T(8,128)(2,1)}) %reduce-scatter.2.cloned.1.call-update) | async-done | bytes 262160 | tf_op jit(solution)/shard_map/reduce_scatter | solution.py:42
  300.2 8.4 %copy.14 = bf16[2048,2048]{1,0:T(8,128)(2,1)} copy(bf16[2048,2048]{1,0:T(8,128)(2,1)} %all-gather.4.cloned.1.call-done) | data formatting | bytes 16777216
  308.7 8.4 %copy.15 = bf16[2048,2048]{1,0:T(8,128)(2,1)} copy(bf16[2048,2048]{1,0:T(8,128)(2,1)} %all-gather.6.cloned.1.call-done) | data formatting | bytes 16777216
  317.1 8.4 %copy.16 = bf16[2048,2048]{1,0:T(8,128)(2,1)} copy(bf16[2048,2048]{1,0:T(8,128)(2,1)} %all-gather.8.cloned.1.call-done) | data formatting | bytes 16777216
  (4 shorter events, 0.1 us)
Async XLA Ops:
  7.2 89.1 %all-gather.4.cloned.1.call-start = ((), (), s32[]{:S(2)}) async-start(), calls=%async_computation.1 | async-start | bytes 9437184 | tf_op jit(solution)/shard_map/all_gather | solution.py:35
  11.4 1.6 copy-start
  11.4 167.6 %all-gather.6.cloned.1.call-start = ((), (), s32[]{:S(2)}) async-start(), calls=%async_computation.2 | async-start | bytes 9437184 | tf_op jit(solution)/shard_map/all_gather | solution.py:36
  12.1 2.0 copy-start.2
  12.2 2.1 copy-start.3
  12.2 2.1 copy-start.1
  12.2 249.6 %all-gather.8.cloned.1.call-start = ((), (), s32[]{:S(2)}) async-start(), calls=%async_computation.3 | async-start | bytes 9437184 | tf_op jit(solution)/shard_map/all_gather | solution.py:37
  14.1 286.1 %reduce-scatter.2.cloned.1.call-start = ((), (), s32[]{:S(2)}) async-start(), calls=%async_computation.4 | async-start | bytes 1310720 | tf_op jit(solution)/shard_map/reduce_scatter | solution.py:42
Sparse Core Ops, SparseCore 0:
  11.5 84.7 all-gather.3
  98.5 80.5 all-gather.5
  181.2 80.5 all-gather.7
  273.8 26.4 reduce-scatter.1
where the time goes:
time: 332 us
  waiting for transfers between devices  269 us (81%)
  local copies, waits for them, and re-layouts  26.1 us (8%)
  matrix products  17.6 us (5%)
  between operations  13.8 us (4%)
  other arithmetic  5.63 us (2%)
    all_gather x1, waiting for transfers between devices, on_device(): lax.all_gather(down_local, 'fs', axis=0, tiled=True)  82.7 us
    all_gather x1, waiting for transfers between devices, on_device(): lax.all_gather(gate_local, 'fs', axis=0, tiled=True)  81.7 us
    all_gather x1, waiting for transfers between devices, on_device(): lax.all_gather(up_local, 'fs', axis=0, tiled=True)  76.9 us
    reduce_scatter x1, waiting for transfers between devices, on_device(): lax.psum_scatter(lax.dot_general(down_full, active, (((1,), (1,)), ((), (...  26.6 us
    unnamed x11, local copies, waits for them, and re-layouts  26.1 us
    dot_general x1, matrix products, on_device(): lax.dot_general(down_full, active, (((1,), (1,)), ((), ())), preferred_el...  11.9 us
  transfers between devices with their start and end apart: 4, of which 4 were waited for; matrix products, arithmetic and copies ran while one was open for 2% of the time, Pallas kernels for 0%

commit v1 on v0

v1 whole, which is shorter than its diff:
```python
import functools

import jax
import jax.numpy as jnp
from jax import lax
from jax.experimental import pallas as pl
from jax.experimental.pallas import tpu as pltpu
from jax.sharding import PartitionSpec as P

FF = 2048
CORES = 2

EPSILON = 1e-06
CLAMP_LIMIT = 7.0
SIGMOID_SCALE = 1.702
MESH = pl.DeviceIdType.MESH
LEFT, RIGHT, PARTNER = range(3)


def clamped_unit(pre_gate, pre_up):
    gated = jnp.minimum(pre_gate, CLAMP_LIMIT)
    upper = jnp.clip(pre_up, -CLAMP_LIMIT, CLAMP_LIMIT)
    return gated * jax.nn.sigmoid(SIGMOID_SCALE * gated) * (upper + 1.0)


def kernel(
    n_fs, n_tp, chunk,
    tokens, routes, logits, gain, gate_w, up_w, down_w,
    gate_out, up_out, down_out, moe_out,
    staged, gain_col, normed, acc, active, part, landed,
    load_sem, send_sem, recv_sem, part_send, part_recv,
):
    me, tp = lax.axis_index("fs"), lax.axis_index("tp")
    z, core = me // CORES, me % CORES
    n_z = n_fs // CORES
    partner = z * CORES + (1 - core)
    weights, outs = (gate_w, up_w, down_w), (gate_out, up_out, down_out)
    rows, cols = gate_w.shape
    n_tokens, width = tokens.shape
    n_chunks = rows // chunk
    per_owner = width // n_tp

    barrier = pltpu.get_barrier_semaphore()

    def greet(device):
        pl.semaphore_signal(barrier, inc=1, device_id=device, device_id_type=MESH)

    pl.when(z > 0)(lambda: greet({"fs": me - CORES}))
    pl.when(z < n_z - 1)(lambda: greet({"fs": me + CORES}))
    greet({"fs": partner})
    for step in range(1, n_tp):
        greet({"tp": lax.rem(tp + step, n_tp)})

    def load(a, r):
        return pltpu.make_async_copy(
            weights[a].at[pl.ds(r * chunk, chunk)],
            staged.at[a, pl.ds(r * chunk, chunk)],
            load_sem.at[a, r],
        )

    for a in range(3):
        for r in range(n_chunks):
            load(a, r).start()

    here = lax.broadcasted_iota(jnp.int32, (rows, rows), 0)
    there = lax.broadcasted_iota(jnp.int32, (rows, rows), 1)
    gain_col[...] = jnp.sum(
        jnp.where(here == there, jnp.broadcast_to(gain[...], (rows, rows)), 0.0),
        axis=1, keepdims=True,
    )

    def place(s, r):
        return pl.ds(pl.multiple_of(s * rows + r * chunk, chunk), chunk)

    def copy(kind, a, s, r):
        target = (me - CORES, me + CORES, partner)[kind]
        return pltpu.make_async_remote_copy(
            src_ref=outs[a].at[place(s, r)],
            dst_ref=outs[a].at[place(s, r)],
            send_sem=send_sem.at[kind, a, s // CORES, r],
            recv_sem=recv_sem.at[a, s, r],
            device_id={"fs": target},
            device_id_type=MESH,
        )

    def send_own(a, r):
        pl.when(z > 0)(lambda: copy(LEFT, a, me, r).start())
        pl.when(z < n_z - 1)(lambda: copy(RIGHT, a, me, r).start())
        copy(PARTNER, a, me, r).start()

    own = [(a, r) for a in range(3) for r in range(n_chunks)]
    for i, (a, r) in enumerate(own):
        load(a, r).wait()
        block = staged[a, r * chunk : (r + 1) * chunk, :]
        if a < 2:
            block = gain_col[r * chunk : (r + 1) * chunk, :] * block
        outs[a][place(me, r), :] = block.astype(jnp.bfloat16)
        if i == 0:
            pl.semaphore_wait(
                barrier,
                n_tp + (z > 0).astype(jnp.int32) + (z < n_z - 1).astype(jnp.int32),
            )
        else:
            send_own(*own[i - 1])

    tile = min(32, n_tokens)

    def norm_tile(i, carry):
        at = pl.ds(pl.multiple_of(i * tile, tile), tile)
        wide = tokens[at, :].astype(jnp.float32)
        scale = lax.rsqrt(jnp.mean(wide * wide, axis=-1, keepdims=True) + EPSILON)
        value = (wide * scale).astype(jnp.bfloat16)
        for s in range(n_fs):
            normed[s, at, :] = value[:, s * rows : (s + 1) * rows]
        acc[0, at, :] = jnp.zeros((tile, cols), jnp.float32)
        acc[1, at, :] = jnp.zeros((tile, cols), jnp.float32)
        return carry

    lax.fori_loop(0, 1, norm_tile, 0)
    send_own(*own[-1])
    lax.fori_loop(1, n_tokens // tile, norm_tile, 0)

    wide_tile = min(512, cols)

    def project(a, s):
        block = pl.ds(pl.multiple_of(s * rows, rows), rows)

        def one(i, carry):
            at = pl.ds(pl.multiple_of(i * wide_tile, wide_tile), wide_tile)
            acc[a, :, at] += jnp.dot(
                normed[s], outs[a][block, at], preferred_element_type=jnp.float32
            )
            return carry

        lax.fori_loop(0, cols // wide_tile, one, 0)

    def wait_partner_line(a, s, r):
        copy(PARTNER, a, s, r).wait_recv()

    def wait_partner_block(a, s):
        def one(r, carry):
            wait_partner_line(a, s, r)
            return carry

        lax.fori_loop(0, n_chunks, one, 0)

    def project_pair(a, at_z):
        project(a, at_z * CORES + core)
        other = at_z * CORES + 1 - core
        wait_partner_block(a, other)
        project(a, other)

    def part_copy(s, r):
        start = s * rows + r * chunk
        owner, offset = start // per_owner, start % per_owner
        return pltpu.make_async_remote_copy(
            src_ref=part.at[pl.ds(pl.multiple_of(start, chunk), chunk)],
            dst_ref=landed.at[tp, pl.ds(pl.multiple_of(offset, chunk), chunk)],
            send_sem=part_send.at[s, r],
            recv_sem=part_recv.at[tp, offset // chunk],
            device_id={"tp": owner},
            device_id_type=MESH,
        )

    def down_rows(s, first, count):
        start = s * rows + first * chunk
        size = count * chunk
        at = pl.ds(pl.multiple_of(start, size), size)
        value = lax.dot_general(
            outs[2][at, :], active[...], (((1,), (1,)), ((), ())),
            preferred_element_type=jnp.float32,
        ).astype(jnp.bfloat16)
        owner, offset = start // per_owner, start % per_owner

        @pl.when(owner == tp)
        def _():
            landed[tp, pl.ds(pl.multiple_of(offset, size), size), :] = value

        @pl.when(owner != tp)
        def _():
            part[at, :] = value
            for r in range(count):
                part_copy(s, first + r).start()

    def activate():
        expert = tp * cols // FF

        def one(i, carry):
            at = pl.ds(pl.multiple_of(i * tile, tile), tile)
            score = logits[at, :]
            grown = jnp.exp(score - jnp.max(score, axis=-1, keepdims=True))
            shares = grown / jnp.sum(grown, axis=-1, keepdims=True)
            weight = jnp.sum(
                jnp.where(routes[at, :] == expert, shares, 0.0), axis=-1, keepdims=True
            )
            active[at, :] = (weight * clamped_unit(acc[0, at, :], acc[1, at, :])).astype(
                jnp.bfloat16
            )
            return carry

        lax.fori_loop(0, n_tokens // tile, one, 0)

    def down_near(s, carry):
        at_z = s // CORES

        @pl.when(jnp.abs(at_z - z) < n_z - 1)
        def _():
            pl.when(s % CORES != core)(lambda: wait_partner_block(2, s))
            down_rows(s, 0, n_chunks)

        return carry

    for a in range(2):
        project_pair(a, z)

    for d in range(1, n_z):
        last = d == n_z - 1
        for a in range(3):
            if last and a == 2:
                activate()
                lax.fori_loop(0, n_fs, down_near, 0)

            def arrive(r, carry, a=a, d=d, last=last):
                for sign, inside, onward, more in (
                    (-1, z - d >= 0, RIGHT, z < n_z - 1),
                    (1, z + d < n_z, LEFT, z > 0),
                ):

                    @pl.when(inside)
                    def _():
                        at_z = z + sign * d
                        s = at_z * CORES + core
                        copy(onward, a, s, r).wait_recv()
                        pl.when(more)(lambda: copy(onward, a, s, r).start())
                        copy(PARTNER, a, s, r).start()
                        if last and a == 2:
                            other = at_z * CORES + 1 - core
                            down_rows(s, r, 1)
                            wait_partner_line(a, other, r)
                            down_rows(other, r, 1)

                return carry

            lax.fori_loop(0, n_chunks, arrive, 0)
            if a < 2:
                pl.when(z - d >= 0)(lambda a=a, d=d: project_pair(a, z - d))
                pl.when(z + d < n_z)(lambda a=a, d=d: project_pair(a, z + d))

    for step in range(1, n_tp):
        sender = lax.rem(tp + step, n_tp)
        for j in range(per_owner // chunk):
            spot = landed.at[sender, pl.ds(j * chunk, chunk)]
            pltpu.make_async_remote_copy(
                src_ref=spot, dst_ref=spot, send_sem=part_send.at[0, 0],
                recv_sem=part_recv.at[sender, j],
                device_id={"tp": sender}, device_id_type=MESH,
            ).wait_recv()
    total = landed[0].astype(jnp.float32)
    for p in range(1, n_tp):
        total += landed[p].astype(jnp.float32)
    moe_out[...] = jnp.transpose(total).astype(jnp.bfloat16)

    def sent(s, carry):
        at_z = s // CORES

        def one(r, carry):
            @pl.when(s % CORES == core)
            def _():
                for a in range(3):
                    copy(PARTNER, a, s, r).wait_send()
                    pl.when((z > 0) & (at_z >= z))(lambda: copy(LEFT, a, s, r).wait_send())
                    pl.when((z < n_z - 1) & (at_z <= z))(
                        lambda: copy(RIGHT, a, s, r).wait_send()
                    )

            @pl.when((s * rows + r * chunk) // per_owner != tp)
            def _():
                part_copy(s, r).wait_send()

            return carry

        return lax.fori_loop(0, n_chunks, one, carry)

    lax.fori_loop(0, n_fs, sent, 0)


def write_out(*refs):
    count = (len(refs) - 1) // 2
    sources, targets, sem = refs[:count], refs[count:-1], refs[-1]
    copies = [
        pltpu.make_async_copy(source, target, sem.at[i])
        for i, (source, target) in enumerate(zip(sources, targets))
    ]
    for copy in copies:
        copy.start()
    for copy in copies:
        copy.wait()


def on_device(n_fs, n_tp, tokens, routes, logits, gain, gate_w, up_w, down_w):
    rows, cols = gate_w.shape
    n_tokens, width = tokens.shape
    per_owner = width // n_tp
    chunk = min(64, rows, per_owner)
    n_chunks = rows // chunk
    full = pltpu.VMEM((rows * n_fs, cols), jnp.bfloat16)
    vmem = pl.BlockSpec(memory_space=pltpu.VMEM)
    hbm = pl.BlockSpec(memory_space=pl.ANY)
    held = pl.pallas_call(
        functools.partial(kernel, n_fs, n_tp, chunk),
        out_shape=(full, full, full, pltpu.VMEM((n_tokens, per_owner), jnp.bfloat16)),
        in_specs=[vmem] * 4 + [hbm] * 3,
        out_specs=(vmem,) * 4,
        scratch_shapes=[
            pltpu.VMEM((3, rows, cols), jnp.float32),
            pltpu.VMEM((rows, 1), jnp.float32),
            pltpu.VMEM((n_fs, n_tokens, rows), jnp.bfloat16),
            pltpu.VMEM((2, n_tokens, cols), jnp.float32),
            pltpu.VMEM((n_tokens, cols), jnp.bfloat16),
            pltpu.VMEM((width, n_tokens), jnp.bfloat16),
            pltpu.VMEM((n_tp, per_owner, n_tokens), jnp.bfloat16),
            pltpu.SemaphoreType.DMA((3, n_chunks)),
            pltpu.SemaphoreType.DMA((3, 3, n_fs // CORES, n_chunks)),
            pltpu.SemaphoreType.DMA((3, n_fs, n_chunks)),
            pltpu.SemaphoreType.DMA((n_fs, n_chunks)),
            pltpu.SemaphoreType.DMA((n_tp, per_owner // chunk)),
        ],
        compiler_params=pltpu.CompilerParams(
            collective_id=0, has_side_effects=True, vmem_limit_bytes=34 * 2**20
        ),
    )(tokens, routes, logits, gain.reshape(1, rows), gate_w, up_w, down_w)
    return tuple(pl.pallas_call(
        write_out,
        out_shape=tuple(jax.ShapeDtypeStruct(x.shape, x.dtype) for x in held),
        in_specs=[hbm] * 4,
        out_specs=(hbm,) * 4,
        scratch_shapes=[pltpu.SemaphoreType.DMA((4,))],
        compiler_params=pltpu.CompilerParams(vmem_limit_bytes=2**20),
    )(*held))


def solution(mesh):
    return jax.shard_map(
        functools.partial(on_device, mesh.shape["fs"], mesh.shape["tp"]),
        mesh=mesh,
        in_specs=(
            P("fs", None),
            P("fs", None),
            P("fs", None),
            P("fs"),
            P("fs", "tp"),
            P("fs", "tp"),
            P("fs", "tp"),
        ),
        out_specs=(P(None, "tp"), P(None, "tp"), P(None, "tp"), P("fs", "tp")),
        check_vma=False,
    )
```

time: 332 us -> 229 us (0.69)
  waiting for transfers between devices: 269 us -> 0 us
  Pallas kernels: 0 us -> 224 us
  local copies, waits for them, and re-layouts: 26.1 us -> 2.95 us
  matrix products: 17.6 us -> 0 us
  between operations: 13.8 us -> 0.64 us
  other arithmetic: 5.63 us -> 0 us
    all_gather x3 -> x0, waiting for transfers between devices: 241 us -> none  [the longest x1 82.7 us: on_device(): lax.all_gather(down_local, 'fs', axis=0, tiled=True)]
    pallas_call x0 -> x2, Pallas kernels: none -> 224 us  [the longest x1 215 us: on_device(): pl.pallas_call(functools.partial(kernel, n_fs, n_tp, chunk), out_shape=(f...]
    reduce_scatter x1 -> x0, waiting for transfers between devices: 26.6 us -> none  [on_device(): lax.psum_scatter(lax.dot_general(down_full, active, (((1,), (1,)), ((), (...]
    unnamed x11 -> x2, local copies, waits for them, and re-layouts: 26.1 us -> 2.95 us
    dot_general x2 -> x0, matrix products: 17.6 us -> none  [the longest x1 11.9 us: on_device(): lax.dot_general(down_full, active, (((1,), (1,)), ((), ())), preferred_el...]
    convert_element_type x2 -> x0, other arithmetic: 5.26 us -> none  [the longest x1 4.15 us: on_device(): up_local = (norm_gain[:, None] * up_weight).astype(jnp.bfloat16)]
  transfers between devices with their start and end apart: 4 -> 0, of which waited for: 4 -> 0; matrix products, arithmetic and copies ran while one was open for 2% -> 0% of each run, Pallas kernels for 0% -> 0%
where the time goes in v1:
time: 229 us; the launch traced here: 228 us
  Pallas kernels  224 us (98%)
  local copies, waits for them, and re-layouts  2.95 us (1%)
    pallas_call x1, Pallas kernels, on_device(): pl.pallas_call(functools.partial(kernel, n_fs, n_tp, chunk), out_shape=(f...  215 us
    pallas_call x1, Pallas kernels, on_device(): pl.pallas_call(write_out, out_shape=tuple((jax.ShapeDtypeStruct(x.shape,...  8.72 us

profile of v1, /device:TPU:0, one launch (start us, length us, event | category | flops | bytes accessed | tf_op | source)
XLA Modules:
  0.0 227.7 jit_solution(1701329331480067339)
XLA Ops:
  0.6 1.5 copy.11.routes
  2.1 1.5 copy.12.logits
  3.6 215.3 %shard_map.102 = (bf16[2048,2048]{1,0:T(8,128)(2,1)S(1)}, bf16[2048,2048]{1,0:T(8,128)(2,1)S(1)}, bf16[2048,2048]{1,0:T(8,128)(2,1)S(1)}, bf16[256,512]{1,0:T(8,128)(2,1)S(1)}) custom-call(bf16[256,2048]{1,0:T(8,128)(2,1)} %tokens.1, s32[256,2]{1,0:T(8,128)} %copy.11.routes, f32[256,2]{1,0:T(8,128)} %copy.12.logits, f32[1,256]{1,0:T(1,128)} %bitcast.1, ...), custom_call_target="tpu_custom_call" | custom-call | tf_op jit(solution)/shard_map/pallas_call | solution.py:309
  218.9 8.7 %shard_map.103 = (bf16[2048,2048]{1,0:T(8,128)(2,1)}, bf16[2048,2048]{1,0:T(8,128)(2,1)}, bf16[2048,2048]{1,0:T(8,128)(2,1)}, bf16[256,512]{1,0:T(8,128)(2,1)}) custom-call(bf16[2048,2048]{1,0:T(8,128)(2,1)S(1)} %get-tuple-element.8.refs_0_, bf16[2048,2048]{1,0:T(8,128)(2,1)S(1)} %get-tuple-element.9.refs_1_, ...), custom_call_target="tpu_custom_call" | custom-call | tf_op jit(solution)/shard_map/pallas_call | solution.py:332

commit v2 on v1

v2 whole, which is shorter than its diff:
```python
import functools
import math

import jax
import jax.numpy as jnp
from jax import lax
from jax.experimental import pallas as pl
from jax.experimental.pallas import tpu as pltpu
from jax.sharding import PartitionSpec as P

FF = 2048
CORES = 2

EPSILON = 1e-06
CLAMP_LIMIT = 7.0
SIGMOID_SCALE = 1.702
MESH = pl.DeviceIdType.MESH
LEFT, RIGHT, PARTNER = range(3)


def clamped_unit(pre_gate, pre_up):
    gated = jnp.minimum(pre_gate, CLAMP_LIMIT)
    upper = jnp.clip(pre_up, -CLAMP_LIMIT, CLAMP_LIMIT)
    return gated * jax.nn.sigmoid(SIGMOID_SCALE * gated) * (upper + 1.0)


def as_column(row):
    n = row.shape[1]
    here = lax.broadcasted_iota(jnp.int32, (n, n), 0)
    there = lax.broadcasted_iota(jnp.int32, (n, n), 1)
    spread = jnp.where(here == there, jnp.broadcast_to(row, (n, n)), 0.0)
    return jnp.sum(spread, axis=1, keepdims=True)


def cuts(rows):
    if rows % 256:
        return [[(0, rows)]] * 3
    tables = []
    for parts in ((1, 2, 2, 3), (2, 2, 2, 2), (2, 2, 3, 1)):
        table, start = [], 0
        for part in parts:
            table.append((start, part * rows // 8))
            start += part * rows // 8
        tables.append(table)
    return tables


def kernel(
    n_fs, n_tp,
    tokens, routes, logits, gain, gate_w, up_w, down_w,
    gate_out, up_out, down_out, moe_out,
    staged, gain_col, weight_col, normed, acc, active, part, landed,
    load_sem, send_sem, recv_sem, part_send, part_recv,
):
    me, tp = lax.axis_index("fs"), lax.axis_index("tp")
    z, core = me // CORES, me % CORES
    n_z = n_fs // CORES
    partner = z * CORES + (1 - core)
    weights, outs = (gate_w, up_w, down_w), (gate_out, up_out, down_out)
    rows, cols = gate_w.shape
    n_tokens, width = tokens.shape
    table = cuts(rows)
    n_chunks = len(table[0])
    per_owner = width // n_tp

    barrier = pltpu.get_barrier_semaphore()

    def greet(device):
        pl.semaphore_signal(barrier, inc=1, device_id=device, device_id_type=MESH)

    pl.when(z > 0)(lambda: greet({"fs": me - CORES}))
    pl.when(z < n_z - 1)(lambda: greet({"fs": me + CORES}))
    greet({"fs": partner})
    for step in range(1, n_tp):
        greet({"tp": lax.rem(tp + step, n_tp)})

    def load(a, r):
        return pltpu.make_async_copy(
            weights[a].at[pl.ds(*table[a][r])],
            staged.at[a, pl.ds(*table[a][r])],
            load_sem.at[a, r],
        )

    for a in range(3):
        for r in range(n_chunks):
            load(a, r).start()

    gain_col[...] = as_column(gain[...])

    def place(a, s, r):
        first, size = table[a][r]
        return pl.ds(pl.multiple_of(s * rows + first, math.gcd(rows, first)), size)

    def copy(kind, a, s, r):
        target = (me - CORES, me + CORES, partner)[kind]
        return pltpu.make_async_remote_copy(
            src_ref=outs[a].at[place(a, s, r)],
            dst_ref=outs[a].at[place(a, s, r)],
            send_sem=send_sem.at[kind, a, s // CORES, r],
            recv_sem=recv_sem.at[a, s, r],
            device_id={"fs": target},
            device_id_type=MESH,
        )

    def send_own(a, r):
        pl.when(z > 0)(lambda: copy(LEFT, a, me, r).start())
        pl.when(z < n_z - 1)(lambda: copy(RIGHT, a, me, r).start())
        copy(PARTNER, a, me, r).start()

    own = [(a, r) for a in range(3) for r in range(n_chunks)]
    for i, (a, r) in enumerate(own):
        load(a, r).wait()
        at = pl.ds(*table[a][r])
        block = staged[a, at, :]
        if a < 2:
            block = gain_col[at, :] * block
        outs[a][place(a, me, r), :] = block.astype(jnp.bfloat16)
        if i == 0:
            pl.semaphore_wait(
                barrier,
                n_tp + (z > 0).astype(jnp.int32) + (z < n_z - 1).astype(jnp.int32),
            )
        else:
            send_own(*own[i - 1])

    tile = min(32, n_tokens)

    def norm_tile(i, carry):
        at = pl.ds(pl.multiple_of(i * tile, tile), tile)
        wide = tokens[at, :].astype(jnp.float32)
        scale = lax.rsqrt(jnp.mean(wide * wide, axis=-1, keepdims=True) + EPSILON)
        value = (wide * scale).astype(jnp.bfloat16)
        for s in range(n_fs):
            normed[s, at, :] = value[:, s * rows : (s + 1) * rows]
        acc[0, at, :] = jnp.zeros((tile, cols), jnp.float32)
        acc[1, at, :] = jnp.zeros((tile, cols), jnp.float32)
        return carry

    lax.fori_loop(0, 1, norm_tile, 0)
    send_own(*own[-1])
    lax.fori_loop(1, n_tokens // tile, norm_tile, 0)

    expert = tp * cols // FF
    top = logits.shape[0]
    score = [logits[k : k + 1, :] for k in range(top)]
    peak = functools.reduce(jnp.maximum, score)
    grown = [jnp.exp(x - peak) for x in score]
    whole = sum(grown)
    weight_col[...] = as_column(
        sum(jnp.where(routes[k : k + 1, :] == expert, grown[k] / whole, 0.0) for k in range(top))
    )

    wide_tile = min(512, cols)

    def project(a, s):
        block = pl.ds(pl.multiple_of(s * rows, rows), rows)

        def one(i, carry):
            at = pl.ds(pl.multiple_of(i * wide_tile, wide_tile), wide_tile)
            acc[a, :, at] += jnp.dot(
                normed[s], outs[a][block, at], preferred_element_type=jnp.float32
            )
            return carry

        lax.fori_loop(0, cols // wide_tile, one, 0)

    def wait_partner_line(a, s, r):
        copy(PARTNER, a, s, r).wait_recv()

    def wait_partner_block(a, s):
        for r in range(n_chunks):
            wait_partner_line(a, s, r)

    def project_pair(a, at_z):
        project(a, at_z * CORES + core)
        other = at_z * CORES + 1 - core
        wait_partner_block(a, other)
        project(a, other)

    def part_copy(s, r):
        first, size = table[2][r]
        start = s * rows + first
        owner, offset = start // per_owner, start % per_owner
        step = math.gcd(rows, first)
        return pltpu.make_async_remote_copy(
            src_ref=part.at[pl.ds(pl.multiple_of(start, step), size)],
            dst_ref=landed.at[tp, pl.ds(pl.multiple_of(offset, step), size)],
            send_sem=part_send.at[s, r],
            recv_sem=part_recv.at[tp, offset // rows, r],
            device_id={"tp": owner},
            device_id_type=MESH,
        )

    def down_rows(s, chunks):
        first, size = table[2][chunks[0]][0], sum(table[2][r][1] for r in chunks)
        start = s * rows + first
        step = math.gcd(rows, first)
        at = pl.ds(pl.multiple_of(start, step), size)
        value = lax.dot_general(
            outs[2][at, :], active[...], (((1,), (1,)), ((), ())),
            preferred_element_type=jnp.float32,
        ).astype(jnp.bfloat16)
        owner, offset = start // per_owner, start % per_owner

        @pl.when(owner == tp)
        def _():
            landed[tp, pl.ds(pl.multiple_of(offset, step), size), :] = value

        @pl.when(owner != tp)
        def _():
            part[at, :] = value
            for r in chunks:
                part_copy(s, r).start()

    def activate():
        def one(i, carry):
            at = pl.ds(pl.multiple_of(i * tile, tile), tile)
            active[at, :] = (
                weight_col[at, :] * clamped_unit(acc[0, at, :], acc[1, at, :])
            ).astype(jnp.bfloat16)
            return carry

        lax.fori_loop(0, n_tokens // tile, one, 0)

    def down_near(s, carry):
        at_z = s // CORES

        @pl.when(jnp.abs(at_z - z) < n_z - 1)
        def _():
            pl.when(s % CORES != core)(lambda: wait_partner_block(2, s))
            down_rows(s, range(n_chunks))

        return carry

    for a in range(2):
        project_pair(a, z)

    for d in range(1, n_z):
        last = d == n_z - 1
        for a in range(3):
            if last and a == 2:
                activate()
                lax.fori_loop(0, n_fs, down_near, 0)

            def arrive(r, a=a, d=d, last=last):
                for sign, inside, onward, more in (
                    (-1, z - d >= 0, RIGHT, z < n_z - 1),
                    (1, z + d < n_z, LEFT, z > 0),
                ):

                    @pl.when(inside)
                    def _():
                        at_z = z + sign * d
                        s = at_z * CORES + core
                        copy(onward, a, s, r).wait_recv()
                        pl.when(more)(lambda: copy(onward, a, s, r).start())
                        copy(PARTNER, a, s, r).start()
                        if last and a == 2:
                            other = at_z * CORES + 1 - core
                            down_rows(s, (r,))
                            wait_partner_line(a, other, r)
                            down_rows(other, (r,))

            for r in range(n_chunks):
                arrive(r)
            if a < 2:
                pl.when(z - d >= 0)(lambda a=a, d=d: project_pair(a, z - d))
                pl.when(z + d < n_z)(lambda a=a, d=d: project_pair(a, z + d))

    def sent(s, carry):
        at_z = s // CORES

        @pl.when(s % CORES == core)
        def _():
            for a in range(3):
                for r in range(n_chunks):
                    copy(PARTNER, a, s, r).wait_send()

            @pl.when((z > 0) & (at_z >= z))
            def _():
                for a in range(3):
                    for r in range(n_chunks):
                        copy(LEFT, a, s, r).wait_send()

            @pl.when((z < n_z - 1) & (at_z <= z))
            def _():
                for a in range(3):
                    for r in range(n_chunks):
                        copy(RIGHT, a, s, r).wait_send()

        @pl.when(s * rows // per_owner != tp)
        def _():
            for r in range(n_chunks):
                part_copy(s, r).wait_send()

        return carry

    lax.fori_loop(0, n_fs, sent, 0)

    group = min(128, rows)
    done = 0
    for r in range(n_chunks):
        first, size = table[2][r]
        for j in range(per_owner // rows):
            for step in range(1, n_tp):
                sender = lax.rem(tp + step, n_tp)
                spot = landed.at[sender, pl.ds(j * rows + first, size)]
                pltpu.make_async_remote_copy(
                    src_ref=spot, dst_ref=spot, send_sem=part_send.at[0, 0],
                    recv_sem=part_recv.at[sender, j, r],
                    device_id={"tp": sender}, device_id_type=MESH,
                ).wait_recv()
        while done + group <= first + size:
            for j in range(per_owner // rows):
                at = slice(j * rows + done, j * rows + done + group)
                total = landed[0, at, :].astype(jnp.float32)
                for p in range(1, n_tp):
                    total += landed[p, at, :].astype(jnp.float32)
                moe_out[:, at] = jnp.transpose(total).astype(jnp.bfloat16)
            done += group


def write_out(*refs):
    count = (len(refs) - 1) // 2
    sources, targets, sem = refs[:count], refs[count:-1], refs[-1]
    copies = [
        pltpu.make_async_copy(source, target, sem.at[i])
        for i, (source, target) in enumerate(zip(sources, targets))
    ]
    for copy in copies:
        copy.start()
    for copy in copies:
        copy.wait()


def on_device(n_fs, n_tp, tokens, routes, logits, gain, gate_w, up_w, down_w):
    rows, cols = gate_w.shape
    n_tokens, width = tokens.shape
    per_owner = width // n_tp
    n_chunks = len(cuts(rows)[0])
    full = pltpu.VMEM((rows * n_fs, cols), jnp.bfloat16)
    vmem = pl.BlockSpec(memory_space=pltpu.VMEM)
    hbm = pl.BlockSpec(memory_space=pl.ANY)
    held = pl.pallas_call(
        functools.partial(kernel, n_fs, n_tp),
        out_shape=(full, full, full, pltpu.VMEM((n_tokens, per_owner), jnp.bfloat16)),
        in_specs=[vmem] * 4 + [hbm] * 3,
        out_specs=(vmem,) * 4,
        scratch_shapes=[
            pltpu.VMEM((3, rows, cols), jnp.float32),
            pltpu.VMEM((rows, 1), jnp.float32),
            pltpu.VMEM((n_tokens, 1), jnp.float32),
            pltpu.VMEM((n_fs, n_tokens, rows), jnp.bfloat16),
            pltpu.VMEM((2, n_tokens, cols), jnp.float32),
            pltpu.VMEM((n_tokens, cols), jnp.bfloat16),
            pltpu.VMEM((width, n_tokens), jnp.bfloat16),
            pltpu.VMEM((n_tp, per_owner, n_tokens), jnp.bfloat16),
            pltpu.SemaphoreType.DMA((3, n_chunks)),
            pltpu.SemaphoreType.DMA((3, 3, n_fs // CORES, n_chunks)),
            pltpu.SemaphoreType.DMA((3, n_fs, n_chunks)),
            pltpu.SemaphoreType.DMA((n_fs, n_chunks)),
            pltpu.SemaphoreType.DMA((n_tp, per_owner // rows, n_chunks)),
        ],
        compiler_params=pltpu.CompilerParams(
            collective_id=0, has_side_effects=True, vmem_limit_bytes=34 * 2**20
        ),
    )(tokens, routes.T, logits.T, gain.reshape(1, rows), gate_w, up_w, down_w)
    return tuple(pl.pallas_call(
        write_out,
        out_shape=tuple(jax.ShapeDtypeStruct(x.shape, x.dtype) for x in held),
        in_specs=[hbm] * 4,
        out_specs=(hbm,) * 4,
        scratch_shapes=[pltpu.SemaphoreType.DMA((4,))],
        compiler_params=pltpu.CompilerParams(vmem_limit_bytes=2**20),
    )(*held))


def solution(mesh):
    return jax.shard_map(
        functools.partial(on_device, mesh.shape["fs"], mesh.shape["tp"]),
        mesh=mesh,
        in_specs=(
            P("fs", None),
            P("fs", None),
            P("fs", None),
            P("fs"),
            P("fs", "tp"),
            P("fs", "tp"),
            P("fs", "tp"),
        ),
        out_specs=(P(None, "tp"), P(None, "tp"), P(None, "tp"), P("fs", "tp")),
        check_vma=False,
    )
```

time: 229 us -> 226 us (0.987)
  local copies, waits for them, and re-layouts: 2.95 us -> 0 us
    unnamed x2 -> x0, local copies, waits for them, and re-layouts: 2.95 us -> none
where the time goes in v2:
time: 226 us
  Pallas kernels  225 us (100%)
    pallas_call x1, Pallas kernels, on_device(): pl.pallas_call(functools.partial(kernel, n_fs, n_tp), out_shape=(full, fu...  216 us
    pallas_call x1, Pallas kernels, on_device(): pl.pallas_call(write_out, out_shape=tuple((jax.ShapeDtypeStruct(x.shape,...  8.72 us

profile of v2, /device:TPU:0, one launch (start us, length us, event | category | flops | bytes accessed | tf_op | source)
XLA Modules:
  0.0 225.7 jit_solution(17889904051060069652)
XLA Ops:
  0.6 216.4 %shard_map.102 = (bf16[2048,2048]{1,0:T(8,128)(2,1)S(1)}, bf16[2048,2048]{1,0:T(8,128)(2,1)S(1)}, bf16[2048,2048]{1,0:T(8,128)(2,1)S(1)}, bf16[256,512]{1,0:T(8,128)(2,1)S(1)}) custom-call(bf16[256,2048]{1,0:T(8,128)(2,1)} %tokens.1, s32[2,256]{1,0:T(2,128)} %bitcast.3, f32[2,256]{1,0:T(2,128)} %bitcast.4, f32[1,256]{1,0:T(1,128)} %bitcast.5, ...), custom_call_target="tpu_custom_call" | custom-call | tf_op jit(solution)/shard_map/pallas_call | solution.py:344
  217.0 8.7 %shard_map.103 = (bf16[2048,2048]{1,0:T(8,128)(2,1)}, bf16[2048,2048]{1,0:T(8,128)(2,1)}, bf16[2048,2048]{1,0:T(8,128)(2,1)}, bf16[256,512]{1,0:T(8,128)(2,1)}) custom-call(bf16[2048,2048]{1,0:T(8,128)(2,1)S(1)} %get-tuple-element.8.refs_0_, bf16[2048,2048]{1,0:T(8,128)(2,1)S(1)} %get-tuple-element.9.refs_1_, ...), custom_call_target="tpu_custom_call" | custom-call | tf_op jit(solution)/shard_map/pallas_call | solution.py:368

commit v3 on v2

--- a/solution.py
+++ b/solution.py
@@ -196,9 +196,8 @@
         start = s * rows + first
         step = math.gcd(rows, first)
         at = pl.ds(pl.multiple_of(start, step), size)
-        value = lax.dot_general(
-            outs[2][at, :], active[...], (((1,), (1,)), ((), ())),
-            preferred_element_type=jnp.float32,
+        value = jnp.dot(
+            outs[2][at, :], active[...], preferred_element_type=jnp.float32
         ).astype(jnp.bfloat16)
         owner, offset = start // per_owner, start % per_owner
 
@@ -213,14 +212,17 @@
                 part_copy(s, r).start()
 
     def activate():
+        token_tile = min(128, n_tokens)
+        col_tiles = cols // wide_tile
+
         def one(i, carry):
-            at = pl.ds(pl.multiple_of(i * tile, tile), tile)
-            active[at, :] = (
-                weight_col[at, :] * clamped_unit(acc[0, at, :], acc[1, at, :])
-            ).astype(jnp.bfloat16)
+            at = pl.ds(pl.multiple_of(i // col_tiles * token_tile, token_tile), token_tile)
+            to = pl.ds(pl.multiple_of(i % col_tiles * wide_tile, wide_tile), wide_tile)
+            value = weight_col[at, :] * clamped_unit(acc[0, at, to], acc[1, at, to])
+            active[to, at] = jnp.transpose(value).astype(jnp.bfloat16)
             return carry
 
-        lax.fori_loop(0, n_tokens // tile, one, 0)
+        lax.fori_loop(0, n_tokens // token_tile * col_tiles, one, 0)
 
     def down_near(s, carry):
         at_z = s // CORES
@@ -352,7 +354,7 @@
             pltpu.VMEM((n_tokens, 1), jnp.float32),
             pltpu.VMEM((n_fs, n_tokens, rows), jnp.bfloat16),
             pltpu.VMEM((2, n_tokens, cols), jnp.float32),
-            pltpu.VMEM((n_tokens, cols), jnp.bfloat16),
+            pltpu.VMEM((cols, n_tokens), jnp.bfloat16),
             pltpu.VMEM((width, n_tokens), jnp.bfloat16),
             pltpu.VMEM((n_tp, per_owner, n_tokens), jnp.bfloat16),
             pltpu.SemaphoreType.DMA((3, n_chunks)),

time: 226 us -> 225 us (level)
  no operation moved by 1% of the time
where the time goes in v3:
time: 225 us
  Pallas kernels  225 us (100%)
    pallas_call x1, Pallas kernels, on_device(): pl.pallas_call(functools.partial(kernel, n_fs, n_tp), out_shape=(full, fu...  216 us
    pallas_call x1, Pallas kernels, on_device(): pl.pallas_call(write_out, out_shape=tuple((jax.ShapeDtypeStruct(x.shape,...  8.72 us

profile of v3, /device:TPU:0, one launch (start us, length us, event | category | flops | bytes accessed | tf_op | source)
XLA Modules:
  0.0 225.2 jit_solution(10158237579023213281)
XLA Ops:
  0.6 215.8 %shard_map.102 = (bf16[2048,2048]{1,0:T(8,128)(2,1)S(1)}, bf16[2048,2048]{1,0:T(8,128)(2,1)S(1)}, bf16[2048,2048]{1,0:T(8,128)(2,1)S(1)}, bf16[256,512]{1,0:T(8,128)(2,1)S(1)}) custom-call(bf16[256,2048]{1,0:T(8,128)(2,1)} %tokens.1, s32[2,256]{1,0:T(2,128)} %bitcast.3, f32[2,256]{1,0:T(2,128)} %bitcast.4, f32[1,256]{1,0:T(1,128)} %bitcast.5, ...), custom_call_target="tpu_custom_call" | custom-call | tf_op jit(solution)/shard_map/pallas_call | solution.py:346
  216.4 8.7 %shard_map.103 = (bf16[2048,2048]{1,0:T(8,128)(2,1)}, bf16[2048,2048]{1,0:T(8,128)(2,1)}, bf16[2048,2048]{1,0:T(8,128)(2,1)}, bf16[256,512]{1,0:T(8,128)(2,1)}) custom-call(bf16[2048,2048]{1,0:T(8,128)(2,1)S(1)} %get-tuple-element.8.refs_0_, bf16[2048,2048]{1,0:T(8,128)(2,1)S(1)} %get-tuple-element.9.refs_1_, ...), custom_call_target="tpu_custom_call" | custom-call | tf_op jit(solution)/shard_map/pallas_call | solution.py:370
